TPU v7x, 32 devices: a whole 2x2x4 slice. The times are simulated.
32 devices in a mesh: grp: 2 (over y), tp: 4 (over z), dp: 4 (over x, core).
Axes of the slice: x: 2, y: 2, z: 4, core: 2. Of those that a mesh axis runs over, the one named last changes fastest.
Arguments:
- tokens: bfloat16 [128, 4096], P('grp', 'dp'), parts along dimension 0, may hold values from -6 to 6
- norm_gain: float32 [2, 4096], P(None, 'dp'), may hold values from 0.1 to 1.9
- w_query: bfloat16 [2, 4096, 512], P(None, 'dp', 'tp'), may hold values from -0.09375 to 0.09375
- w_key: bfloat16 [2, 4096, 512], P(None, 'dp', 'tp'), may hold values from -0.09375 to 0.09375
- w_value: bfloat16 [2, 4096, 512], P(None, 'dp', 'tp'), may hold values from -0.09375 to 0.09375
- w_outgate: bfloat16 [2, 4096, 512], P(None, 'dp', 'tp'), may hold values from -0.09375 to 0.09375
- gate_weight: bfloat16 [2, 4, 384, 2], P(None, 'tp'), may hold values from -0.3125 to 0.3125
- forget_bias: float32 [2, 4], P(None, 'tp'), may hold values from -2 to 4
- w_mix: bfloat16 [2, 512, 4096], P(None, 'tp', 'dp'), may hold values from -0.25 to 0.25
- memory: float32 [2, 128, 4, 128, 128], P(None, ('grp', 'dp'), 'tp'), parts along dimension 1, may hold values from -3 to 3
- normalizer: float32 [2, 128, 4, 128], P(None, ('grp', 'dp'), 'tp'), parts along dimension 1, may hold values from -3 to 3
- stabilizer: float32 [2, 128, 4], P(None, ('grp', 'dp'), 'tp'), parts along dimension 1, may hold values from -4 to 4
Outputs:
- result: bfloat16 [128, 4096], P('grp', 'dp'), parts along dimension 0
- new_memory: float32 [2, 128, 4, 128, 128], P(None, ('grp', 'dp'), 'tp'), parts along dimension 1
- new_normalizer: float32 [2, 128, 4, 128], P(None, ('grp', 'dp'), 'tp'), parts along dimension 1
- new_stabilizer: float32 [2, 128, 4], P(None, ('grp', 'dp'), 'tp'), parts along dimension 1
There are 2 independent parts, one for each index of `grp`. A program takes and returns all parts, laid end to end along the dimension named above; an argument that names none is the same for every part. Nothing has to cross between parts.
All inputs are finite; a program needn't handle non-finite values.
Results may differ from a plain program's by a relative error of at most 0.018.
Values may be sent and summed in bfloat16 or wider, within the bound.
A program may use at most 64 MiB of HBM per device.

v0:
```python
import jax
import jax.numpy as jnp
from jax import lax
from jax.sharding import PartitionSpec as P

D = 4096
DK = 128
BLOCKS = 2
EPS = 1e-06


def shards(
    tokens,
    norm_gain,
    w_query,
    w_key,
    w_value,
    w_outgate,
    gate_weight,
    forget_bias,
    w_mix,
    memory,
    normalizer,
    stabilizer,
):
    x = tokens
    seq_own = memory.shape[1]
    heads_own = memory.shape[2]
    mems, norms, stabs = ([], [], [])
    for blk in range(BLOCKS):
        xf = x.astype(jnp.float32)
        squares = jnp.sum(xf * xf, axis=-1)
        scaled_in = (xf * norm_gain[blk]).astype(jnp.bfloat16)
        terms = tuple(
            (
                jnp.dot(scaled_in, weight[blk], preferred_element_type=jnp.float32)
                for weight in (w_query, w_key, w_value, w_outgate)
            )
        )
        totals = lax.psum(squares, "dp")
        summed = lax.psum_scatter(terms, "dp", scatter_dimension=0, tiled=True)
        own_squares = lax.dynamic_slice_in_dim(totals, lax.axis_index("dp") * seq_own, seq_own, 0)
        scale = lax.rsqrt(own_squares / D + EPS)
        projs = [
            (scale[:, None] * part)
            .astype(jnp.bfloat16)
            .astype(jnp.float32)
            .reshape(seq_own, heads_own, DK)
            for part in summed
        ]
        query, key, value, outgate = projs
        joined = jnp.concatenate([query, key, value], axis=-1)
        pre = jnp.einsum(
            "shc,hcg->shg",
            joined,
            gate_weight[blk].astype(jnp.float32),
            precision=lax.Precision.HIGHEST,
        )
        log_input = pre[..., 0]
        log_forget = jax.nn.log_sigmoid(pre[..., 1] + forget_bias[blk])
        stab = stabilizer[blk]
        new_stab = jnp.maximum(log_forget + stab, log_input)
        keep = jnp.exp(log_forget + stab - new_stab)
        admit = jnp.exp(log_input - new_stab)
        scaled_key = key * DK ** (-0.5)
        new_mem = (
            keep[..., None, None] * memory[blk]
            + admit[..., None, None] * scaled_key[..., :, None] * value[..., None, :]
        )
        new_norm = keep[..., None] * normalizer[blk] + admit[..., None] * scaled_key
        numer = jnp.einsum("shd,shde->she", query, new_mem, precision=lax.Precision.HIGHEST)
        denom = jnp.maximum(jnp.abs(jnp.sum(query * new_norm, axis=-1)), 1.0)
        readout = numer / denom[..., None]
        gated = (
            (readout * jax.nn.sigmoid(outgate))
            .reshape(seq_own, heads_own * DK)
            .astype(jnp.bfloat16)
        )
        mix_weight = w_mix[blk]
        partial_mix = jnp.dot(
            lax.all_gather(gated, "dp", axis=0, tiled=True),
            mix_weight,
            preferred_element_type=jnp.float32,
        )
        mine = lax.psum_scatter(partial_mix, "tp", scatter_dimension=0, tiled=True)
        row_count = mine.shape[0]
        own_rows = lax.dynamic_slice_in_dim(xf, lax.axis_index("tp") * row_count, row_count, 0)
        updated = (own_rows + mine).astype(jnp.bfloat16)
        x = lax.all_gather(updated, "tp", axis=0, tiled=True)
        mems.append(new_mem)
        norms.append(new_norm)
        stabs.append(new_stab)
    return (x, jnp.stack(mems, axis=0), jnp.stack(norms, axis=0), jnp.stack(stabs, axis=0))


def solution(mesh):
    in_specs = (
        P("grp", "dp"),
        P(None, "dp"),
        P(None, "dp", "tp"),
        P(None, "dp", "tp"),
        P(None, "dp", "tp"),
        P(None, "dp", "tp"),
        P(None, "tp", None, None),
        P(None, "tp"),
        P(None, "tp", "dp"),
        P(None, ("grp", "dp"), "tp", None, None),
        P(None, ("grp", "dp"), "tp", None),
        P(None, ("grp", "dp"), "tp"),
    )
    out_specs = (
        P("grp", "dp"),
        P(None, ("grp", "dp"), "tp", None, None),
        P(None, ("grp", "dp"), "tp", None),
        P(None, ("grp", "dp"), "tp"),
    )
    return jax.shard_map(shards, mesh=mesh, in_specs=in_specs, out_specs=out_specs, check_vma=False)
```

profile of v0, /device:TPU:0, one launch (start us, length us, event | category | flops | bytes accessed | tf_op | source)
XLA Modules:
  0.0 279.2 jit_solution(203216173123310671)
XLA Ops:
  7.3 0.9 fusion.116
  8.2 1.8 fusion.32
  10.1 1.8 fusion.30
  12.0 1.8 fusion.34
  13.8 1.8 fusion.28
  15.7 1.0 multiply_reduce_fusion.1
  16.8 8.4 %psum.14 = f32[64]{0:T(128)S(1)} all-reduce(f32[64]{0:T(128)S(1)} %multiply_reduce_fusion.1), channel_id=1, replica_groups=mesh['grp'=2,'tp'=4,'dp'=4] {'dp'}, use_global_device_ids=true, to_apply=%region_1.0 | all-reduce | flops 64 | bytes 512 | tf_op jit(solution)/shard_map/psum | solution.py:40
  25.1 0.6 fusion.117
  25.8 7.5 %reduce-scatter.13.cloned.1.call-done = f32[16,128]{1,0:T(8,128)} async-done(((f32[64,128]{1,0:T(8,128)}), f32[16,128]{1,0:T(8,128)}) %reduce-scatter.13.cloned.1.call-update) | async-done | bytes 8208 | tf_op jit(solution)/shard_map/reduce_scatter | solution.py:41
  33.3 22.0 %reduce-scatter.15.cloned.1.call-done = f32[16,128]{1,0:T(8,128)} async-done(((f32[64,128]{1,0:T(8,128)}), f32[16,128]{1,0:T(8,128)}) %reduce-scatter.15.cloned.1.call-update) | async-done | bytes 8208 | tf_op jit(solution)/shard_map/reduce_scatter | solution.py:41
  55.3 22.5 %reduce-scatter.11.cloned.1.call-done = f32[16,128]{1,0:T(8,128)} async-done(((f32[64,128]{1,0:T(8,128)}), f32[16,128]{1,0:T(8,128)}) %reduce-scatter.11.cloned.1.call-update) | async-done | bytes 8208 | tf_op jit(solution)/shard_map/reduce_scatter | solution.py:41
  77.8 0.8 convert_bitcast_fusion.3
  78.8 0.7 fusion.70
  79.4 0.7 fusion.108
  80.4 0.8 fusion.4
  81.1 18.6 %reduce-scatter.17.cloned.1.call-done = f32[16,128]{1,0:T(8,128)} async-done(((f32[64,128]{1,0:T(8,128)}), f32[16,128]{1,0:T(8,128)}) %reduce-scatter.17.cloned.1.call-update) | async-done | bytes 8208 | tf_op jit(solution)/shard_map/reduce_scatter | solution.py:41
  99.7 0.8 multiply_convert_fusion.15
  100.5 5.2 %all_gather.12 = bf16[64,128]{1,0:T(8,128)(2,1)S(1)} all-gather(bf16[16,128]{1,0:T(8,128)(2,1)S(1)} %multiply_convert_fusion.15), channel_id=1, replica_groups=mesh['grp'=2,'tp'=4,'dp'=4] {'dp'}, dimensions={0}, use_global_device_ids=true | all-gather | bytes 20480 | tf_op jit(solution)/shard_map/all_gather | solution.py:81
  105.7 0.9 fusion.26
  106.7 20.1 %reduce-scatter.19.cloned.1.call-done = f32[16,1024]{1,0:T(8,128)} async-done(((f32[64,1024]{1,0:T(8,128)}), f32[16,1024]{1,0:T(8,128)}) %reduce-scatter.19.cloned.1.call-update) | async-done | bytes 65552 | tf_op jit(solution)/shard_map/reduce_scatter | solution.py:85
  126.8 0.8 add_convert_fusion.1
  127.6 13.4 %all_gather.13 = bf16[64,1024]{1,0:T(8,128)(2,1)S(1)} all-gather(bf16[16,1024]{1,0:T(8,128)(2,1)S(1)} %add_convert_fusion.1), channel_id=1, replica_groups=mesh['grp'=2,'tp'=4,'dp'=4] {'tp'}, dimensions={0}, use_global_device_ids=true | all-gather | bytes 163840 | tf_op jit(solution)/shard_map/all_gather | solution.py:89
  141.0 1.7 fusion.22
  142.7 1.7 fusion.20
  144.5 1.7 fusion.18
  146.3 1.7 fusion.24
  148.2 5.7 %psum.15 = f32[64]{0:T(128)S(1)} all-reduce(f32[64]{0:T(128)S(1)} %multiply_reduce_fusion), channel_id=1, replica_groups=mesh['grp'=2,'tp'=4,'dp'=4] {'dp'}, use_global_device_ids=true, to_apply=%region_9.10 | all-reduce | flops 64 | bytes 512 | tf_op jit(solution)/shard_map/psum | solution.py:40
  154.1 0.6 reduce-scatter.27.cloned.1.call-update
  154.7 9.3 %reduce-scatter.23.cloned.1.call-done = f32[16,128]{1,0:T(8,128)} async-done(((f32[64,128]{1,0:T(8,128)}), f32[16,128]{1,0:T(8,128)}) %reduce-scatter.23.cloned.1.call-update) | async-done | bytes 8208 | tf_op jit(solution)/shard_map/reduce_scatter | solution.py:41
  164.0 22.0 %reduce-scatter.25.cloned.1.call-done = f32[16,128]{1,0:T(8,128)} async-done(((f32[64,128]{1,0:T(8,128)}), f32[16,128]{1,0:T(8,128)}) %reduce-scatter.25.cloned.1.call-update) | async-done | bytes 8208 | tf_op jit(solution)/shard_map/reduce_scatter | solution.py:41
  186.0 22.5 %reduce-scatter.21.cloned.1.call-done = f32[16,128]{1,0:T(8,128)} async-done(((f32[64,128]{1,0:T(8,128)}), f32[16,128]{1,0:T(8,128)}) %reduce-scatter.21.cloned.1.call-update) | async-done | bytes 8208 | tf_op jit(solution)/shard_map/reduce_scatter | solution.py:41
  208.5 0.8 convert_bitcast_fusion.2
  209.5 1.3 bitcast_maximum_fusion.2
  210.8 0.7 fusion.74
  211.5 0.7 fusion.106
  212.4 0.8 fusion.1
  213.1 17.4 %reduce-scatter.27.cloned.1.call-done = f32[16,128]{1,0:T(8,128)} async-done(((f32[64,128]{1,0:T(8,128)}), f32[16,128]{1,0:T(8,128)}) %reduce-scatter.27.cloned.1.call-update) | async-done | bytes 8208 | tf_op jit(solution)/shard_map/reduce_scatter | solution.py:41
  230.5 0.8 multiply_convert_fusion.10
  231.3 5.2 %all_gather.14 = bf16[64,128]{1,0:T(8,128)(2,1)S(1)} all-gather(bf16[16,128]{1,0:T(8,128)(2,1)S(1)} %multiply_convert_fusion.10), channel_id=1, replica_groups=mesh['grp'=2,'tp'=4,'dp'=4] {'dp'}, dimensions={0}, use_global_device_ids=true | all-gather | bytes 20480 | tf_op jit(solution)/shard_map/all_gather | solution.py:81
  236.5 0.9 fusion.16
  237.4 0.6 pad_maximum_fusion.1
  238.0 0.6 pad_maximum_fusion.2
  238.6 0.7 multiply_add_fusion.1
  239.3 1.5 pad_maximum_fusion
  240.8 16.8 %reduce-scatter.29.cloned.1.call-done = f32[16,1024]{1,0:T(8,128)} async-done(((f32[64,1024]{1,0:T(8,128)}), f32[16,1024]{1,0:T(8,128)}) %reduce-scatter.29.cloned.1.call-update) | async-done | bytes 65552 | tf_op jit(solution)/shard_map/reduce_scatter | solution.py:85
  257.5 0.8 add_convert_fusion
  258.4 13.4 %all_gather.15 = bf16[64,1024]{1,0:T(8,128)(2,1)S(1)} all-gather(bf16[16,1024]{1,0:T(8,128)(2,1)S(1)} %add_convert_fusion), channel_id=1, replica_groups=mesh['grp'=2,'tp'=4,'dp'=4] {'tp'}, dimensions={0}, use_global_device_ids=true | all-gather | bytes 163840 | tf_op jit(solution)/shard_map/all_gather | solution.py:89
  271.7 0.7 copy.28
  (48 shorter events, 1.6 us)
Async XLA Ops:
  7.2 18.0 %copy-start.5 = (f32[2,1]{0,1:T(1,128)S(1)}, f32[2,1]{0,1:T(1,128)}, u32[]{:S(2)}) copy-start(f32[2,1]{0,1:T(1,128)} %param.19) | copy-start | bytes 28
  7.2 71.5 %copy-start.6 = (bf16[2,1,384,2]{2,3,1,0:T(2,128)(2,1)S(1)}, bf16[2,1,384,2]{2,3,1,0:T(2,128)(2,1)}, u32[]{:S(2)}) copy-start(bf16[2,1,384,2]{2,3,1,0:T(2,128)(2,1)} %param.18) | copy-start | bytes 9220
  7.2 71.6 %copy-start.4 = (f32[2,16,1]{1,2,0:T(1,128)S(1)}, f32[2,16,1]{1,2,0:T(1,128)}, u32[]{:S(2)}) copy-start(f32[2,16,1]{1,2,0:T(1,128)} %param.23) | copy-start | bytes 388
  7.2 73.0 %copy-start.3 = (f32[2,16,1,128]{3,2,1,0:T(1,128)S(1)}, f32[2,16,1,128]{3,2,1,0:T(1,128)}, u32[]{:S(2)}) copy-start(f32[2,16,1,128]{3,2,1,0:T(1,128)} %param.22) | copy-start | bytes 49156
  7.2 73.1 %copy-start = (f32[2,16,1,128,128]{4,3,2,1,0:T(8,128)S(1)}, f32[2,16,1,128,128]{4,3,2,1,0:T(8,128)}, u32[]{:S(2)}) copy-start(f32[2,16,1,128,128]{4,3,2,1,0:T(8,128)} %param.21) | copy-start | bytes 6291460
  7.2 98.5 %copy-start.2 = (bf16[2,128,1024]{2,1,0:T(8,128)(2,1)S(1)}, bf16[2,128,1024]{2,1,0:T(8,128)(2,1)}, u32[]{:S(2)}) copy-start(bf16[2,128,1024]{2,1,0:T(8,128)(2,1)} %param.20) | copy-start | bytes 1572868
  7.2 26.1 %reduce-scatter.13.cloned.1.call-start = ((), (), s32[]{:S(2)}) async-start(), calls=%async_computation.11 | async-start | bytes 40960 | tf_op jit(solution)/shard_map/reduce_scatter | solution.py:41
  8.1 98.5 %copy-start.1 = (bf16[64,1024]{1,0:T(8,128)(2,1)S(1)}, bf16[64,1024]{1,0:T(8,128)(2,1)}, u32[]{:S(2)}) copy-start(bf16[64,1024]{1,0:T(8,128)(2,1)} %param.12) | copy-start | bytes 393220
  10.0 45.3 %reduce-scatter.15.cloned.1.call-start = ((), (), s32[]{:S(2)}) async-start(), calls=%async_computation.12 | async-start | bytes 40960 | tf_op jit(solution)/shard_map/reduce_scatter | solution.py:41
  11.9 65.9 %reduce-scatter.11.cloned.1.call-start = ((), (), s32[]{:S(2)}) async-start(), calls=%async_computation.10 | async-start | bytes 40960 | tf_op jit(solution)/shard_map/reduce_scatter | solution.py:41
  13.8 85.9 %reduce-scatter.17.cloned.1.call-start = ((), (), s32[]{:S(2)}) async-start(), calls=%async_computation.13 | async-start | bytes 40960 | tf_op jit(solution)/shard_map/reduce_scatter | solution.py:41
  15.7 111.1 %reduce-scatter.19.cloned.1.call-start = ((), (), s32[]{:S(2)}) async-start(), calls=%async_computation.14 | async-start | bytes 327680 | tf_op jit(solution)/shard_map/reduce_scatter | solution.py:85
  106.6 57.5 %reduce-scatter.23.cloned.1.call-start = ((), (), s32[]{:S(2)}) async-start(), calls=%async_computation.16 | async-start | bytes 40960 | tf_op jit(solution)/shard_map/reduce_scatter | solution.py:41
  146.2 39.8 %reduce-scatter.25.cloned.1.call-start = ((), (), s32[]{:S(2)}) async-start(), calls=%async_computation.17 | async-start | bytes 40960 | tf_op jit(solution)/shard_map/reduce_scatter | solution.py:41
  148.1 60.5 %reduce-scatter.21.cloned.1.call-start = ((), (), s32[]{:S(2)}) async-start(), calls=%async_computation.15 | async-start | bytes 40960 | tf_op jit(solution)/shard_map/reduce_scatter | solution.py:41
  153.9 76.6 %reduce-scatter.27.cloned.1.call-start = ((), (), s32[]{:S(2)}) async-start(), calls=%async_computation.18 | async-start | bytes 40960 | tf_op jit(solution)/shard_map/reduce_scatter | solution.py:41
  154.7 102.9 %reduce-scatter.29.cloned.1.call-start = ((), (), s32[]{:S(2)}) async-start(), calls=%async_computation.19 | async-start | bytes 327680 | tf_op jit(solution)/shard_map/reduce_scatter | solution.py:85
Sparse Core Ops, SparseCore 0:
  11.0 22.2 reduce-scatter.12
  35.7 19.5 reduce-scatter.14
  58.3 19.5 reduce-scatter.10
  80.1 19.5 reduce-scatter.16
  106.7 19.9 reduce-scatter.18
  146.3 17.6 reduce-scatter.22
  166.5 19.5 reduce-scatter.24
  189.0 19.5 reduce-scatter.20
  210.9 19.5 reduce-scatter.26
  237.5 19.9 reduce-scatter.28
where the time goes:
time: 280 us; the launch traced here: 279 us
  waiting for transfers between devices  179 us (64%)
  blocking collectives  51.2 us (18%)
  matrix products  17.7 us (6%)
  between operations  14.3 us (5%)
  other arithmetic  14 us (5%)
    reduce_scatter x8, waiting for transfers between devices, shards(): summed = lax.psum_scatter(terms, 'dp', scatter_dimension=0, tiled=True)  142 us
    reduce_scatter x2, waiting for transfers between devices, shards(): mine = lax.psum_scatter(partial_mix, 'tp', scatter_dimension=0, tiled=True)  36.9 us
    all_gather x2, blocking collectives, shards(): x = lax.all_gather(updated, 'tp', axis=0, tiled=True)  26.7 us
    dot_general x8, matrix products, shards(): jnp.dot(scaled_in, weight[blk], preferred_element_type=jnp.float32)  14.2 us
    psum x2, blocking collectives, shards(): totals = lax.psum(squares, 'dp')  14 us
    all_gather x2, blocking collectives, shards(): lax.all_gather(gated, 'dp', axis=0, tiled=True)  10.4 us
  transfers between devices with their start and end apart: 10, of which 10 were waited for; matrix products, arithmetic and copies ran while one was open for 7% of the time, Pallas kernels for 0%

commit v1 on v0

--- a/solution.py
+++ b/solution.py
@@ -86,7 +86,14 @@
         row_count = mine.shape[0]
         own_rows = lax.dynamic_slice_in_dim(xf, lax.axis_index("tp") * row_count, row_count, 0)
         updated = (own_rows + mine).astype(jnp.bfloat16)
-        x = lax.all_gather(updated, "tp", axis=0, tiled=True)
+        ways, here = (lax.axis_size("tp"), lax.axis_index("tp"))
+        x, reach = (updated, 1)
+        while reach < ways:
+            theirs = lax.ppermute(x, "tp", [(d, d ^ reach) for d in range(ways)])
+            mine_first = jnp.concatenate([x, theirs], axis=0)
+            theirs_first = jnp.concatenate([theirs, x], axis=0)
+            x = jnp.where(here & reach == 0, mine_first, theirs_first)
+            reach = 2 * reach
         mems.append(new_mem)
         norms.append(new_norm)
         stabs.append(new_stab)

time: 280 us -> 269 us (0.961)
  blocking collectives: 51.2 us -> 24.4 us
  waiting for transfers between devices: 179 us -> 193 us
    all_gather x2 -> x0, blocking collectives: 26.7 us -> none  [shards(): x = lax.all_gather(updated, 'tp', axis=0, tiled=True)]
    ppermute x0 -> x4, waiting for transfers between devices: none -> 16 us  [shards(): theirs = lax.ppermute(x, 'tp', [(d, d ^ reach) for d in range(ways)])]
  transfers between devices with their start and end apart: 10 -> 14, of which waited for: 10 -> 14; matrix products, arithmetic and copies ran while one was open for 7% -> 9% of each run, Pallas kernels for 0% -> 0%
where the time goes in v1:
time: 269 us; the launch traced here: 268 us
  waiting for transfers between devices  193 us (72%)
  blocking collectives  24.4 us (9%)
  matrix products  17.8 us (7%)
  other arithmetic  14.8 us (6%)
  between operations  14.4 us (5%)
    reduce_scatter x8, waiting for transfers between devices, shards(): summed = lax.psum_scatter(terms, 'dp', scatter_dimension=0, tiled=True)  140 us
    reduce_scatter x2, waiting for transfers between devices, shards(): mine = lax.psum_scatter(partial_mix, 'tp', scatter_dimension=0, tiled=True)  36.7 us
    ppermute x4, waiting for transfers between devices, shards(): theirs = lax.ppermute(x, 'tp', [(d, d ^ reach) for d in range(ways)])  16 us
    dot_general x8, matrix products, shards(): jnp.dot(scaled_in, weight[blk], preferred_element_type=jnp.float32)  14.2 us
    psum x2, blocking collectives, shards(): totals = lax.psum(squares, 'dp')  14 us
    all_gather x2, blocking collectives, shards(): lax.all_gather(gated, 'dp', axis=0, tiled=True)  10.4 us
  transfers between devices with their start and end apart: 14, of which 14 were waited for; matrix products, arithmetic and copies ran while one was open for 9% of the time, Pallas kernels for 0%

profile of v1, /device:TPU:0, one launch (start us, length us, event | category | flops | bytes accessed | tf_op | source)
XLA Modules:
  0.0 268.3 jit_solution(12830532220922849592)
XLA Ops:
  7.3 0.9 fusion.117
  8.2 1.8 fusion.32
  10.1 1.8 fusion.30
  11.9 1.8 fusion.34
  13.8 1.8 fusion.28
  15.7 1.0 multiply_reduce_fusion.1
  16.8 8.4 %psum.14 = f32[64]{0:T(128)S(1)} all-reduce(f32[64]{0:T(128)S(1)} %multiply_reduce_fusion.1), channel_id=1, replica_groups=mesh['grp'=2,'tp'=4,'dp'=4] {'dp'}, use_global_device_ids=true, to_apply=%region_1.0 | all-reduce | flops 64 | bytes 512 | tf_op jit(solution)/shard_map/psum | solution.py:40
  25.8 7.5 %reduce-scatter.13.cloned.1.call-done = f32[16,128]{1,0:T(8,128)} async-done(((f32[64,128]{1,0:T(8,128)}), f32[16,128]{1,0:T(8,128)}) %reduce-scatter.13.cloned.1.call-update) | async-done | bytes 8208 | tf_op jit(solution)/shard_map/reduce_scatter | solution.py:41
  33.3 22.0 %reduce-scatter.15.cloned.1.call-done = f32[16,128]{1,0:T(8,128)} async-done(((f32[64,128]{1,0:T(8,128)}), f32[16,128]{1,0:T(8,128)}) %reduce-scatter.15.cloned.1.call-update) | async-done | bytes 8208 | tf_op jit(solution)/shard_map/reduce_scatter | solution.py:41
  55.3 22.5 %reduce-scatter.11.cloned.1.call-done = f32[16,128]{1,0:T(8,128)} async-done(((f32[64,128]{1,0:T(8,128)}), f32[16,128]{1,0:T(8,128)}) %reduce-scatter.11.cloned.1.call-update) | async-done | bytes 8208 | tf_op jit(solution)/shard_map/reduce_scatter | solution.py:41
  77.8 0.8 convert_bitcast_fusion.3
  78.8 0.7 fusion.71
  79.4 0.7 fusion.109
  80.4 0.8 fusion.4
  81.1 18.6 %reduce-scatter.17.cloned.1.call-done = f32[16,128]{1,0:T(8,128)} async-done(((f32[64,128]{1,0:T(8,128)}), f32[16,128]{1,0:T(8,128)}) %reduce-scatter.17.cloned.1.call-update) | async-done | bytes 8208 | tf_op jit(solution)/shard_map/reduce_scatter | solution.py:41
  99.7 0.8 multiply_convert_fusion.11
  100.5 5.2 %all_gather.6 = bf16[64,128]{1,0:T(8,128)(2,1)S(1)} all-gather(bf16[16,128]{1,0:T(8,128)(2,1)S(1)} %multiply_convert_fusion.11), channel_id=1, replica_groups=mesh['grp'=2,'tp'=4,'dp'=4] {'dp'}, dimensions={0}, use_global_device_ids=true | all-gather | bytes 20480 | tf_op jit(solution)/shard_map/all_gather | solution.py:81
  105.7 0.9 fusion.26
  106.7 20.1 %reduce-scatter.19.cloned.1.call-done = f32[16,1024]{1,0:T(8,128)} async-done(((f32[64,1024]{1,0:T(8,128)}), f32[16,1024]{1,0:T(8,128)}) %reduce-scatter.19.cloned.1.call-update) | async-done | bytes 65552 | tf_op jit(solution)/shard_map/reduce_scatter | solution.py:85
  126.8 0.8 add_convert_fusion.1
  127.7 4.0 %collective-permute-done = bf16[16,1024]{1,0:T(8,128)(2,1)S(1)} collective-permute-done((bf16[16,1024]{1,0:T(8,128)(2,1)S(1)}, bf16[16,1024]{1,0:T(8,128)(2,1)S(1)}, u32[]{:S(2)}, u32[]{:S(2)}) %collective-permute-start) | collective-permute-done | bytes 32800 | tf_op jit(solution)/shard_map/ppermute | solution.py:92
  131.7 0.9 collective-permute-start.1
  132.6 4.7 %collective-permute-done.1 = bf16[32,1024]{1,0:T(8,128)(2,1)S(1)} collective-permute-done((bf16[32,1024]{1,0:T(8,128)(2,1)S(1)}, bf16[32,1024]{1,0:T(8,128)(2,1)S(1)}, u32[]{:S(2)}, u32[]{:S(2)}) %collective-permute-start.1) | collective-permute-done | bytes 65568 | tf_op jit(solution)/shard_map/ppermute | solution.py:92
  137.3 1.7 fusion.22
  139.1 1.7 fusion.20
  141.0 1.8 fusion.24
  142.9 5.7 %psum.15 = f32[64]{0:T(128)S(1)} all-reduce(f32[64]{0:T(128)S(1)} %multiply_reduce_fusion), channel_id=1, replica_groups=mesh['grp'=2,'tp'=4,'dp'=4] {'dp'}, use_global_device_ids=true, to_apply=%region_9.10 | all-reduce | flops 64 | bytes 512 | tf_op jit(solution)/shard_map/psum | solution.py:40
  148.6 1.7 fusion.18
  150.5 6.4 %reduce-scatter.23.cloned.1.call-done = f32[16,128]{1,0:T(8,128)} async-done(((f32[64,128]{1,0:T(8,128)}), f32[16,128]{1,0:T(8,128)}) %reduce-scatter.23.cloned.1.call-update) | async-done | bytes 8208 | tf_op jit(solution)/shard_map/reduce_scatter | solution.py:41
  156.9 22.0 %reduce-scatter.25.cloned.1.call-done = f32[16,128]{1,0:T(8,128)} async-done(((f32[64,128]{1,0:T(8,128)}), f32[16,128]{1,0:T(8,128)}) %reduce-scatter.25.cloned.1.call-update) | async-done | bytes 8208 | tf_op jit(solution)/shard_map/reduce_scatter | solution.py:41
  178.9 22.6 %reduce-scatter.21.cloned.1.call-done = f32[16,128]{1,0:T(8,128)} async-done(((f32[64,128]{1,0:T(8,128)}), f32[16,128]{1,0:T(8,128)}) %reduce-scatter.21.cloned.1.call-update) | async-done | bytes 8208 | tf_op jit(solution)/shard_map/reduce_scatter | solution.py:41
  201.5 0.8 convert_bitcast_fusion.2
  202.4 0.7 fusion.75
  203.1 0.7 fusion.107
  204.0 0.8 fusion.1
  204.7 18.7 %reduce-scatter.27.cloned.1.call-done = f32[16,128]{1,0:T(8,128)} async-done(((f32[64,128]{1,0:T(8,128)}), f32[16,128]{1,0:T(8,128)}) %reduce-scatter.27.cloned.1.call-update) | async-done | bytes 8208 | tf_op jit(solution)/shard_map/reduce_scatter | solution.py:41
  223.5 0.8 multiply_convert_fusion.6
  224.2 5.2 %all_gather.7 = bf16[64,128]{1,0:T(8,128)(2,1)S(1)} all-gather(bf16[16,128]{1,0:T(8,128)(2,1)S(1)} %multiply_convert_fusion.6), channel_id=1, replica_groups=mesh['grp'=2,'tp'=4,'dp'=4] {'dp'}, dimensions={0}, use_global_device_ids=true | all-gather | bytes 20480 | tf_op jit(solution)/shard_map/all_gather | solution.py:81
  229.4 0.9 fusion.16
  230.3 0.8 multiply_add_fusion.1
  231.1 1.5 pad_maximum_fusion
  232.6 1.3 bitcast_maximum_fusion.2
  233.9 16.6 %reduce-scatter.29.cloned.1.call-done = f32[16,1024]{1,0:T(8,128)} async-done(((f32[64,1024]{1,0:T(8,128)}), f32[16,1024]{1,0:T(8,128)}) %reduce-scatter.29.cloned.1.call-update) | async-done | bytes 65552 | tf_op jit(solution)/shard_map/reduce_scatter | solution.py:85
  250.5 0.8 add_convert_fusion
  252.0 3.4 %collective-permute-done.2 = bf16[16,1024]{1,0:T(8,128)(2,1)S(1)} collective-permute-done((bf16[16,1024]{1,0:T(8,128)(2,1)S(1)}, bf16[16,1024]{1,0:T(8,128)(2,1)S(1)}, u32[]{:S(2)}, u32[]{:S(2)}) %collective-permute-start.2) | collective-permute-done | bytes 32800 | tf_op jit(solution)/shard_map/ppermute | solution.py:92
  255.5 0.9 collective-permute-start.3
  257.0 3.8 %collective-permute-done.3 = bf16[32,1024]{1,0:T(8,128)(2,1)S(1)} collective-permute-done((bf16[32,1024]{1,0:T(8,128)(2,1)S(1)}, bf16[32,1024]{1,0:T(8,128)(2,1)S(1)}, u32[]{:S(2)}, u32[]{:S(2)}) %collective-permute-start.3) | collective-permute-done | bytes 65568 | tf_op jit(solution)/shard_map/ppermute | solution.py:92
  260.8 0.7 maximum_select_fusion.1
  (56 shorter events, 3.5 us)
Async XLA Ops:
  7.2 18.0 %copy-start.5 = (f32[2,1]{0,1:T(1,128)S(1)}, f32[2,1]{0,1:T(1,128)}, u32[]{:S(2)}) copy-start(f32[2,1]{0,1:T(1,128)} %param.19) | copy-start | bytes 28
  7.2 71.5 %copy-start.6 = (bf16[2,1,384,2]{2,3,1,0:T(2,128)(2,1)S(1)}, bf16[2,1,384,2]{2,3,1,0:T(2,128)(2,1)}, u32[]{:S(2)}) copy-start(bf16[2,1,384,2]{2,3,1,0:T(2,128)(2,1)} %param.18) | copy-start | bytes 9220
  7.2 71.6 %copy-start.4 = (f32[2,16,1]{1,2,0:T(1,128)S(1)}, f32[2,16,1]{1,2,0:T(1,128)}, u32[]{:S(2)}) copy-start(f32[2,16,1]{1,2,0:T(1,128)} %param.23) | copy-start | bytes 388
  7.2 73.0 %copy-start.3 = (f32[2,16,1,128]{3,2,1,0:T(1,128)S(1)}, f32[2,16,1,128]{3,2,1,0:T(1,128)}, u32[]{:S(2)}) copy-start(f32[2,16,1,128]{3,2,1,0:T(1,128)} %param.22) | copy-start | bytes 49156
  7.2 73.1 %copy-start = (f32[2,16,1,128,128]{4,3,2,1,0:T(8,128)S(1)}, f32[2,16,1,128,128]{4,3,2,1,0:T(8,128)}, u32[]{:S(2)}) copy-start(f32[2,16,1,128,128]{4,3,2,1,0:T(8,128)} %param.21) | copy-start | bytes 6291460
  7.2 98.5 %copy-start.2 = (bf16[2,128,1024]{2,1,0:T(8,128)(2,1)S(1)}, bf16[2,128,1024]{2,1,0:T(8,128)(2,1)}, u32[]{:S(2)}) copy-start(bf16[2,128,1024]{2,1,0:T(8,128)(2,1)} %param.20) | copy-start | bytes 1572868
  7.2 26.1 %reduce-scatter.13.cloned.1.call-start = ((), (), s32[]{:S(2)}) async-start(), calls=%async_computation.11 | async-start | bytes 40960 | tf_op jit(solution)/shard_map/reduce_scatter | solution.py:41
  8.1 98.5 %copy-start.1 = (bf16[64,1024]{1,0:T(8,128)(2,1)S(1)}, bf16[64,1024]{1,0:T(8,128)(2,1)}, u32[]{:S(2)}) copy-start(bf16[64,1024]{1,0:T(8,128)(2,1)} %param.12) | copy-start | bytes 393220
  10.0 45.3 %reduce-scatter.15.cloned.1.call-start = ((), (), s32[]{:S(2)}) async-start(), calls=%async_computation.12 | async-start | bytes 40960 | tf_op jit(solution)/shard_map/reduce_scatter | solution.py:41
  11.9 65.9 %reduce-scatter.11.cloned.1.call-start = ((), (), s32[]{:S(2)}) async-start(), calls=%async_computation.10 | async-start | bytes 40960 | tf_op jit(solution)/shard_map/reduce_scatter | solution.py:41
  13.8 85.9 %reduce-scatter.17.cloned.1.call-start = ((), (), s32[]{:S(2)}) async-start(), calls=%async_computation.13 | async-start | bytes 40960 | tf_op jit(solution)/shard_map/reduce_scatter | solution.py:41
  15.7 111.1 %reduce-scatter.19.cloned.1.call-start = ((), (), s32[]{:S(2)}) async-start(), calls=%async_computation.14 | async-start | bytes 327680 | tf_op jit(solution)/shard_map/reduce_scatter | solution.py:85
  106.6 50.3 %reduce-scatter.23.cloned.1.call-start = ((), (), s32[]{:S(2)}) async-start(), calls=%async_computation.16 | async-start | bytes 40960 | tf_op jit(solution)/shard_map/reduce_scatter | solution.py:41
  127.6 4.1 %collective-permute-start = (bf16[16,1024]{1,0:T(8,128)(2,1)S(1)}, bf16[16,1024]{1,0:T(8,128)(2,1)S(1)}, u32[]{:S(2)}, u32[]{:S(2)}) collective-permute-start(bf16[16,1024]{1,0:T(8,128)(2,1)S(1)} %add_convert_fusion.1), channel_id=1, source_target_pairs={{0,4},{4,0},{8,12},{12,8},{1,5},{5,1},{9,13},{13,9},{2,6},{6,2},{1... | collective-permute-start | bytes 98312 | tf_op jit(solution)/shard_map/ppermute | solution.py:92
  131.7 5.6 %collective-permute-start.1 = (bf16[32,1024]{1,0:T(8,128)(2,1)S(1)}, bf16[32,1024]{1,0:T(8,128)(2,1)S(1)}, u32[]{:S(2)}, u32[]{:S(2)}) collective-permute-start(bf16[32,1024]{1,0:T(8,128)(2,1)S(1)} %maximum_select_fusion.2), channel_id=1, source_target_pairs={{0,8},{4,12},{8,0},{12,4},{1,9},{5,13},{9,1},{13,5},{2,10},{6,14},... | collective-permute-start | bytes 196616 | tf_op jit(solution)/shard_map/ppermute | solution.py:92
  139.1 39.8 %reduce-scatter.25.cloned.1.call-start = ((), (), s32[]{:S(2)}) async-start(), calls=%async_computation.17 | async-start | bytes 40960 | tf_op jit(solution)/shard_map/reduce_scatter | solution.py:41
  140.9 60.6 %reduce-scatter.21.cloned.1.call-start = ((), (), s32[]{:S(2)}) async-start(), calls=%async_computation.15 | async-start | bytes 40960 | tf_op jit(solution)/shard_map/reduce_scatter | solution.py:41
  148.5 74.9 %reduce-scatter.27.cloned.1.call-start = ((), (), s32[]{:S(2)}) async-start(), calls=%async_computation.18 | async-start | bytes 40960 | tf_op jit(solution)/shard_map/reduce_scatter | solution.py:41
  150.4 100.1 %reduce-scatter.29.cloned.1.call-start = ((), (), s32[]{:S(2)}) async-start(), calls=%async_computation.19 | async-start | bytes 327680 | tf_op jit(solution)/shard_map/reduce_scatter | solution.py:85
  251.4 4.1 %collective-permute-start.2 = (bf16[16,1024]{1,0:T(8,128)(2,1)S(1)}, bf16[16,1024]{1,0:T(8,128)(2,1)S(1)}, u32[]{:S(2)}, u32[]{:S(2)}) collective-permute-start(bf16[16,1024]{1,0:T(8,128)(2,1)S(1)} %add_convert_fusion), channel_id=1, source_target_pairs={{0,4},{4,0},{8,12},{12,8},{1,5},{5,1},{9,13},{13,9},{2,6},{6,2},{1... | collective-permute-start | bytes 98312 | tf_op jit(solution)/shard_map/ppermute | solution.py:92
  255.5 5.3 %collective-permute-start.3 = (bf16[32,1024]{1,0:T(8,128)(2,1)S(1)}, bf16[32,1024]{1,0:T(8,128)(2,1)S(1)}, u32[]{:S(2)}, u32[]{:S(2)}) collective-permute-start(bf16[32,1024]{1,0:T(8,128)(2,1)S(1)} %maximum_select_fusion.3), channel_id=1, source_target_pairs={{0,8},{4,12},{8,0},{12,4},{1,9},{5,13},{9,1},{13,5},{2,10},{6,14},... | collective-permute-start | bytes 196616 | tf_op jit(solution)/shard_map/ppermute | solution.py:92
Sparse Core Ops, SparseCore 0:
  11.0 22.2 reduce-scatter.12
  35.7 19.5 reduce-scatter.14
  58.3 19.5 reduce-scatter.10
  80.1 19.5 reduce-scatter.16
  106.7 19.9 reduce-scatter.18
  139.2 17.6 reduce-scatter.22
  159.3 19.5 reduce-scatter.24
  181.9 19.5 reduce-scatter.20
  203.9 19.5 reduce-scatter.26
  230.5 19.9 reduce-scatter.28
